TPU v7x, 256 devices: a whole 4x4x8 slice. The times are simulated.
256 devices in a mesh: sp: 32 (over z, x), tp: 8 (over y, core).
Axes of the slice: x: 4, y: 4, z: 8, core: 2. Of those that a mesh axis runs over, the one named last changes fastest.
Arguments:
- latents: bfloat16 [16384, 2048], P(('sp', 'tp')), may hold values from -6 to 6
- context: bfloat16 [512, 2048], P('sp'), may hold values from -6 to 6
- cond: float32 [2048], P('sp'), may hold values from -6 to 6
- ctx_cond: float32 [2048], P('sp'), may hold values from -6 to 6
- mod_weight: float32 [2048, 6144], P('sp', 'tp'), may hold values from -0.125 to 0.125
- query_weight: bfloat16 [2048, 2048], P(None, 'tp'), may hold values from -1 to 1, as said below
- key_matrix: bfloat16 [2048, 1024], P(None, 'tp'), may hold values from -1 to 1, as said below
- value_matrix: bfloat16 [2048, 1024], P(None, 'tp'), may hold values from -0.125 to 0.125
- out_weight: bfloat16 [2048, 2048], P('tp'), may hold values from -0.125 to 0.125
- query_gain: float32 [128], replicated, may hold values from 0.7 to 7
- key_gain: float32 [128], replicated, may hold values from 0.7 to 7
Outputs:
- updated: bfloat16 [16384, 2048], P(('sp', 'tp'))
Inputs may be any that keep to these rules, and one draw needn't show every extreme that they name: `query_weight`: entries of order 2048 to the power -1/2. `key_matrix`: entries of order 2048 to the power -1/2.
All inputs are finite; a program needn't handle non-finite values.
Results may differ from a plain program's by a relative error of at most 0.0085.
The roundings to bfloat16 on the way count: a program that leaves them out, or rounds other values in their place, can miss the bound.
Values may be sent and summed in bfloat16 or wider, within the bound.
No kernel may reach another device: no remote copies, remote signals or barrier semaphores. Data moves between devices by JAX's collectives and lax.ppermute only.
A program may use at most 128 MiB of HBM per device.

v0:
```python
import math
import jax
import jax.numpy as jnp
from jax import lax
from jax.sharding import Mesh
from jax.sharding import PartitionSpec as P

GRID_W = 64
SP = ("sp_0", "sp_1")
SP_TP = ("sp_0", "sp_1", "tp")
NORM_EPS = 1e-06
ROPE_BASE = 10000.0


def over_axes(value, axes):
    for axis in axes:
        value = lax.psum(value, axis)
    return value


def side_by_side(arrays, axis, dim, along):
    both = jnp.concatenate(arrays, axis=along)
    filled, at, done = (lax.all_gather(both, axis, axis=dim, tiled=True), 0, [])
    for a in arrays:
        done.append(lax.slice_in_dim(filled, at, at + a.shape[along], axis=along))
        at += a.shape[along]
    return tuple(done)


def normalize(latent_value_rows):
    return latent_value_rows * lax.rsqrt(
        jnp.mean(latent_value_rows * latent_value_rows, axis=-1, keepdims=True) + NORM_EPS
    )


def rotate(latent_value_rows, positions):
    quarter = latent_value_rows.shape[-1] // 2
    inv_freq = ROPE_BASE ** (-jnp.arange(quarter, dtype=jnp.float32) / quarter)
    angles = positions.astype(jnp.float32)[:, None] * inv_freq[None, :]
    cos_table = jnp.cos(angles)[:, None, :]
    sin_table = jnp.sin(angles)[:, None, :]
    first, second = (latent_value_rows[..., :quarter], latent_value_rows[..., quarter:])
    return jnp.concatenate(
        [first * cos_table - second * sin_table, second * cos_table + first * sin_table], axis=-1
    )


def axial(latent_value_rows, positions):
    half_dim = latent_value_rows.shape[-1] // 2
    return jnp.concatenate(
        [
            rotate(latent_value_rows[..., :half_dim], positions // GRID_W),
            rotate(latent_value_rows[..., half_dim:], positions % GRID_W),
        ],
        axis=-1,
    )


def modulate(latent_value_rows, mod_row):
    model_width = latent_value_rows.shape[-1]
    shift_vec = mod_row[:model_width]
    scale_vec = mod_row[model_width : 2 * model_width]
    return (
        normalize(latent_value_rows.astype(jnp.float32)) * (1.0 + scale_vec) + shift_vec
    ).astype(jnp.bfloat16)


def body(
    latents,
    context,
    cond,
    ctx_cond,
    mod_weight,
    query_weight,
    key_matrix,
    value_matrix,
    out_weight,
    query_gain,
    key_gain,
):
    model_width = latents.shape[1]
    head_dim = query_gain.shape[0]
    sp_count = lax.axis_size(SP)
    partials = jnp.dot(
        jax.nn.silu(jnp.stack([cond, ctx_cond])), mod_weight, precision=lax.Precision.HIGHEST
    )
    summed = over_axes(partials, SP)
    modulation = lax.all_gather(summed, "tp", axis=1, tiled=True)
    gate_vec = modulation[0, 2 * model_width :]
    normalised_rows = modulate(latents, modulation[0])
    prefix_normalised = modulate(context, modulation[1])
    query_cols = query_weight.shape[1]
    key_cols = key_matrix.shape[1]
    piece = lax.all_gather(normalised_rows, "tp", axis=0, tiled=True)
    projected = jnp.concatenate(
        [
            jnp.dot(piece, query_weight, preferred_element_type=jnp.float32),
            jnp.dot(piece, key_matrix, preferred_element_type=jnp.float32),
            jnp.dot(piece, value_matrix, preferred_element_type=jnp.float32),
        ],
        axis=1,
    )
    row_count = projected.shape[0]
    positions = lax.axis_index(SP) * row_count + jnp.arange(row_count, dtype=jnp.int32)
    query_heads = projected[:, :query_cols].reshape(row_count, -1, head_dim)
    query_heads = axial(normalize(query_heads) * query_gain, positions).astype(jnp.bfloat16)
    key_heads = projected[:, query_cols : query_cols + key_cols].reshape(row_count, -1, head_dim)
    key_heads = axial(normalize(key_heads) * key_gain, positions).astype(jnp.bfloat16)
    value_heads = (
        projected[:, query_cols + key_cols :].reshape(row_count, -1, head_dim).astype(jnp.bfloat16)
    )
    key_part = jnp.dot(prefix_normalised, key_matrix, preferred_element_type=jnp.float32).reshape(
        prefix_normalised.shape[0], -1, head_dim
    )
    value_part = jnp.dot(
        prefix_normalised, value_matrix, preferred_element_type=jnp.float32
    ).reshape(prefix_normalised.shape[0], -1, head_dim)
    local_keys = (normalize(key_part) * key_gain).astype(jnp.bfloat16)
    local_values = value_part.astype(jnp.bfloat16)
    prefix_keys, prefix_values = side_by_side((local_keys, local_values), SP, 0, 1)
    kv_local = key_heads.shape[1]
    group_size = query_heads.shape[1] // kv_local
    grouped = query_heads.reshape(row_count, kv_local, group_size, head_dim).transpose(1, 2, 0, 3)
    grouped = grouped.reshape(kv_local, group_size * row_count, head_dim)
    inv_root = head_dim ** (-0.5)
    lift = math.log(sp_count * row_count / (2.0 * prefix_keys.shape[0]))
    ctx_scores = (
        jnp.einsum("hqd,khd->hqk", grouped, prefix_keys, preferred_element_type=jnp.float32)
        * inv_root
        + lift
    )
    top_init = jnp.max(ctx_scores, axis=-1)
    ctx_weights = jnp.exp(ctx_scores - top_init[..., None])
    initial = (
        top_init,
        jnp.sum(ctx_weights, axis=-1),
        jnp.einsum(
            "hqk,khd->hqd",
            ctx_weights.astype(jnp.bfloat16),
            prefix_values,
            preferred_element_type=jnp.float32,
        ),
    )

    def update(state_now, key_block, value_block):
        top_old, total_old, acc_old = state_now
        scores = (
            jnp.einsum("hqd,khd->hqk", grouped, key_block, preferred_element_type=jnp.float32)
            * inv_root
        )
        top_new = jnp.maximum(top_old, jnp.max(scores, axis=-1))
        factor = jnp.exp(top_old - top_new)
        weights_now = jnp.exp(scores - top_new[..., None])
        acc_new = acc_old * factor[..., None] + jnp.einsum(
            "hqk,khd->hqd",
            weights_now.astype(jnp.bfloat16),
            value_block,
            preferred_element_type=jnp.float32,
        )
        return (top_new, total_old * factor + jnp.sum(weights_now, axis=-1), acc_new)

    key_piece, value_piece = side_by_side((key_heads, value_heads), SP, 0, 1)
    key_count = key_piece.shape[0]
    rows_per_block = math.gcd(key_count, 2048)
    block_count = key_count // rows_per_block
    key_blocks = key_piece.reshape(block_count, rows_per_block, kv_local, head_dim)
    value_blocks = value_piece.reshape(block_count, rows_per_block, kv_local, head_dim)

    def one_step(state_in, blocks_in):
        return (update(state_in, blocks_in[0], blocks_in[1]), None)

    state_out, _ = lax.scan(one_step, initial, (key_blocks, value_blocks))
    top_fin, total_fin, acc_fin = state_out
    attended = (acc_fin / total_fin[..., None]).astype(jnp.bfloat16)
    attended = (
        attended.reshape(kv_local, group_size, row_count, head_dim)
        .transpose(2, 0, 1, 3)
        .reshape(row_count, -1)
    )
    exchanged = lax.all_to_all(attended, "tp", split_axis=0, concat_axis=1, tiled=True)
    mixed_rows = jnp.dot(
        exchanged,
        lax.all_gather(out_weight, "tp", axis=0, tiled=True),
        preferred_element_type=jnp.float32,
    )
    return (latents.astype(jnp.float32) + gate_vec * normalize(mixed_rows)).astype(jnp.bfloat16)


def solution(mesh):
    torus = Mesh(mesh.devices.reshape(8, 4, mesh.shape["tp"]), ("sp_0", "sp_1", "tp"))
    placed = (
        P(SP_TP, None),
        P(SP, None),
        P(SP),
        P(SP),
        P(SP, "tp"),
        P(None, "tp"),
        P(None, "tp"),
        P(None, "tp"),
        P("tp", None),
        P(),
        P(),
    )
    return jax.shard_map(
        body, mesh=torus, in_specs=placed, out_specs=P(SP_TP, None), check_vma=False
    )
```

profile of v0, /device:TPU:1, one launch (start us, length us, event | category | flops | bytes accessed | tf_op | source)
XLA Modules:
  0.0 285.0 jit_solution(6609689054624795851)
XLA Ops:
  7.8 17.5 %psum.14 = f32[2,768]{1,0:T(2,128)S(1)} all-reduce(f32[2,768]{1,0:T(2,128)S(1)} %fusion.67), channel_id=1, replica_groups=mesh['sp_0'=8,'sp_1'=4,'tp'=8] {'sp_0'}, use_global_device_ids=true, to_apply=%region_0.1 | all-reduce | flops 1536 | bytes 12288 | tf_op jit(solution)/shard_map/psum | solution.py:17
  25.3 8.6 %psum.15 = f32[2,768]{1,0:T(2,128)S(1)} all-reduce(f32[2,768]{1,0:T(2,128)S(1)} %psum.14), channel_id=1, replica_groups=mesh['sp_0'=8,'sp_1'=4,'tp'=8] {'sp_1'}, use_global_device_ids=true, to_apply=%region_1.2 | all-reduce | flops 1536 | bytes 12288 | tf_op jit(solution)/shard_map/psum | solution.py:17
  33.9 19.5 %all_gather.15 = f32[2,6144]{1,0:T(2,128)S(1)} all-gather(f32[2,768]{1,0:T(2,128)S(1)} %psum.15), channel_id=1, replica_groups=mesh['sp_0'=8,'sp_1'=4,'tp'=8] {'tp'}, dimensions={1}, use_global_device_ids=true | all-gather | bytes 55296 | tf_op jit(solution)/shard_map/all_gather | solution.py:88
  54.5 1.8 fusion.31
  56.5 23.1 %all-gather.4.cloned.1.call-done = bf16[512,2048]{1,0:T(8,128)(2,1)} async-done(((bf16[64,2048]{1,0:T(8,128)(2,1)}), bf16[512,2048]{1,0:T(8,128)(2,1)}) %all-gather.4.cloned.1.call-update) | async-done | bytes 2097168 | tf_op jit(solution)/shard_map/all_gather | solution.py:94
  79.5 2.5 multiply_reduce_fusion.3
  82.7 2.5 fusion.22
  86.8 3.0 %multiply_cosine_fusion.1 = (f32[512,32]{1,0:T(8,128)S(1)}, f32[512,32]{1,0:T(8,128)}, f32[512,32]{1,0:T(8,128)}, f32[512,32]{1,0:T(8,128)}) fusion(f32[32]{0:T(128)S(1)} %multiply_power_fusion, f32[512]{0:T(512)S(1)} %get-tuple-element.112, f32[512]{0:T(512)S(1)} %get-tuple-element.113), kind=kLoop, calls=%fused_computation.50 | loop fusion | flops 32768 | bytes 266368 | tf_op jit(solution)/shard_map/cos | solution.py:40
  92.6 40.4 %all_gather.17 = bf16[512,2,128]{2,0,1:T(8,128)(2,1)} all-gather(bf16[16,2,128]{2,0,1:T(8,128)(2,1)S(1)} %pad_maximum_fusion.2), channel_id=1, replica_groups=mesh['sp_0'=8,'sp_1'=4,'tp'=8] {'sp_0','sp_1'}, dimensions={0}, use_global_device_ids=true | all-gather | bytes 270336 | tf_op jit(solution)/shard_map/all_gather | solution.py:23
  139.6 46.4 %all-gather.6.cloned.1.call-done = bf16[16384,2,128]{0,2,1:T(8,128)(2,1)} async-done(((bf16[512,2,128]{0,2,1:T(8,128)(2,1)}), bf16[16384,2,128]{0,2,1:T(8,128)(2,1)}) %all-gather.6.cloned.1.call-update) | async-done | bytes 8388624 | tf_op jit(solution)/shard_map/all_gather | solution.py:23
  186.1 5.8 %fusion.76 = (bf16[16384,1,128]{0,2,1:T(8,128)(2,1)}, bf16[16384,1,128]{0,2,1:T(8,128)(2,1)}) fusion(bf16[16384,2,128]{0,2,1:T(8,128)(2,1)} %all-gather.6.cloned.1.call-done), kind=kLoop, calls=%fused_computation.126 | loop fusion | bytes 16777216 | tf_op jit(solution)/shard_map/slice | solution.py:25
  191.9 6.3 %copy.23 = bf16[16384,1,128]{2,0,1:T(8,128)(2,1)} copy(bf16[16384,1,128]{0,2,1:T(8,128)(2,1)} %get-tuple-element.78) | data formatting | bytes 8388608 | tf_op jit(solution)/shard_map/while | solution.py:172
  198.2 6.5 %copy.24 = bf16[16384,1,128]{2,0,1:T(8,128)(2,1)} copy(bf16[16384,1,128]{0,2,1:T(8,128)(2,1)} %get-tuple-element.77) | data formatting | bytes 8388608 | tf_op jit(solution)/shard_map/while | solution.py:172
  204.7 52.6 %while.14 = (s32[]{:T(128)}, f32[1,1024]{1,0:T(1,128)S(1)}, f32[1,1024]{1,0:T(1,128)S(1)}, f32[1,1024,128]{2,1,0:T(8,128)S(1)}, bf16[8,2048,1,128]{3,1,2,0:T(8,1...) while((s32[]{:T(128)}, f32[1,1024]{1,0:T(1,128)S(1)}, ...), condition=%wide.region_12.13_spmd, body=%wide.region_9.12_spmd.sunk | while | flops 1090783232 | bytes 27590756 | solution.py:172
  204.7 2.3 multiply_reduce_fusion.6
  208.5 2.8 fusion.97
  211.3 2.3 multiply_reduce_fusion.6
  215.1 2.8 fusion.97
  217.9 2.3 multiply_reduce_fusion.6
  221.6 2.8 fusion.97
  224.4 2.3 multiply_reduce_fusion.6
  228.2 2.8 fusion.97
  231.0 2.3 multiply_reduce_fusion.6
  234.8 2.8 fusion.97
  237.6 2.3 multiply_reduce_fusion.6
  241.4 2.8 fusion.97
  244.2 2.3 multiply_reduce_fusion.6
  247.9 2.8 fusion.97
  250.7 2.3 multiply_reduce_fusion.6
  254.5 2.8 fusion.97
  258.0 14.5 %all_to_all.19 = bf16[8,64,256]{2,1,0:T(8,128)(2,1)S(1)} all-to-all(bf16[8,64,256]{2,1,0:T(8,128)(2,1)S(1)} %all_to_all.14), channel_id=1, replica_groups=mesh['sp_0'=8,'sp_1'=4,'tp'=8] {'tp'}, dimensions={0} | all-to-all | bytes 524288 | tf_op jit(solution)/shard_map/all_to_all | solution.py:180
  272.5 5.1 %multiply_reduce_fusion.1 = (f32[64]{0:T(128)S(1)}, f32[64,2048]{1,0:T(8,128)S(1)}) fusion(bf16[64,2048]{1,0:T(8,128)(2,1)S(1)} %bitcast.110, bf16[2048,2048]{1,0:T(8,128)(2,1)} %all-gather.8.cloned.1.call-done), kind=kOutput, calls=%fused_computation.39 | convolution fusion | flops 537132992 | bytes 9175296 | tf_op jit(solution)/shard_map/dot_general | solution.py:181
  (85 shorter events, 27.3 us)
Async XLA Ops:
  6.5 126.6 %copy-start = (bf16[2048,256]{1,0:T(8,128)(2,1)S(1)}, bf16[2048,256]{1,0:T(8,128)(2,1)}, u32[]{:S(2)}) copy-start(bf16[2048,256]{1,0:T(8,128)(2,1)} %param.18) | copy-start | bytes 3145732
  6.5 75.5 %copy-start.5 = (f32[128]{0:T(128)S(1)}, f32[128]{0:T(128)}, u32[]{:S(2)}) copy-start(f32[128]{0:T(128)} %param.23) | copy-start | bytes 1540
  6.5 73.0 %all-gather.4.cloned.1.call-start = ((), (), s32[]{:S(2)}) async-start(), calls=%async_computation.1 | async-start | bytes 2359296 | tf_op jit(solution)/shard_map/all_gather | solution.py:94
  56.4 129.7 %all-gather.6.cloned.1.call-start = ((), (), s32[]{:S(2)}) async-start(), calls=%async_computation.2 | async-start | bytes 8650752 | tf_op jit(solution)/shard_map/all_gather | solution.py:23
  56.4 33.3 %copy-start.4 = (bf16[16,2048]{1,0:T(8,128)(2,1)S(1)}, bf16[16,2048]{1,0:T(8,128)(2,1)}, u32[]{:S(2)}) copy-start(bf16[16,2048]{1,0:T(8,128)(2,1)} %param.14) | copy-start | bytes 196612
  82.1 51.0 %copy-start.1 = (bf16[512,2048]{1,0:T(8,128)(2,1)S(1)}, bf16[512,2048]{1,0:T(8,128)(2,1)}, u32[]{:S(2)}) copy-start(bf16[512,2048]{1,0:T(8,128)(2,1)} %all-gather.4.cloned.1.call-done) | copy-start | bytes 6291460
  86.0 49.9 %copy-start.6 = (f32[128]{0:T(128)S(1)}, f32[128]{0:T(128)}, u32[]{:S(2)}) copy-start(f32[128]{0:T(128)} %param.22) | copy-start | bytes 1540
  86.0 186.5 %all-gather.8.cloned.1.call-start = ((), (), s32[]{:S(2)}) async-start(), calls=%async_computation.3 | async-start | bytes 9437184 | tf_op jit(solution)/shard_map/all_gather | solution.py:183
  134.7 3.5 %copy-start.3 = (bf16[512,2,128]{2,0,1:T(8,128)(2,1)S(1)}, bf16[512,2,128]{2,0,1:T(8,128)(2,1)}, u32[]{:S(2)}) copy-start(bf16[512,2,128]{2,0,1:T(8,128)(2,1)} %all_gather.17) | copy-start | bytes 786436
  272.5 5.1 %copy-start.2 = (bf16[64,2048]{1,0:T(8,128)(2,1)S(1)}, bf16[64,2048]{1,0:T(8,128)(2,1)}, u32[]{:S(2)}) copy-start(bf16[64,2048]{1,0:T(8,128)(2,1)} %param.13) | copy-start | bytes 786436
Sparse Core Ops, SparseCore 0:
  56.5 23.0 all-gather.3
  86.1 99.8 all-gather.5
  187.9 54.6 all-gather.7
where the time goes:
time: 286 us; the launch traced here: 285 us
  blocking collectives  100 us (35%)
  waiting for transfers between devices  70.3 us (25%)
  matrix products  57.2 us (20%)
  other arithmetic  22.9 us (8%)
  local copies, waits for them, and re-layouts  20.4 us (7%)
  between operations  13.4 us (5%)
    all_gather x1, waiting for transfers between devices, side_by_side(): filled, at, done = (lax.all_gather(both, axis, axis=dim, tiled=True), 0, [])  46.4 us
    all_gather x1, blocking collectives, side_by_side(): filled, at, done = (lax.all_gather(both, axis, axis=dim, tiled=True), 0, [])  40.4 us
    psum x2, blocking collectives, over_axes(): value = lax.psum(value, axis)  26.1 us
    all_gather x1, waiting for transfers between devices, body(): piece = lax.all_gather(normalised_rows, 'tp', axis=0, tiled=True)  23.1 us
    dot_general x8, matrix products, update(): jnp.einsum('hqk,khd->hqd', weights_now.astype(jnp.bfloat16), value_block,...  22.2 us
    all_gather x1, blocking collectives, body(): modulation = lax.all_gather(summed, 'tp', axis=1, tiled=True)  19.5 us
    dot_general x8, matrix products, update(): jnp.einsum('hqd,khd->hqk', grouped, key_block, preferred_element_type=jnp...  18.4 us
    all_to_all x1, blocking collectives, body(): lax.all_to_all(attended, 'tp', split_axis=0, concat_axis=1, tiled=True)  14.5 us
  transfers between devices with their start and end apart: 3, of which 2 were waited for; matrix products, arithmetic and copies ran while one was open for 29% of the time, Pallas kernels for 0%

commit v1 on v0

--- a/solution.py
+++ b/solution.py
@@ -14,7 +14,7 @@
 
 def over_axes(value, axes):
     for axis in axes:
-        value = lax.psum(value, axis)
+        value = jnp.sum(lax.all_gather(value, axis), axis=0)
     return value
 
 

time: 286 us -> 299 us (1.045)
  blocking collectives: 100 us -> 110 us
    all_gather x0 -> x2, blocking collectives: none -> 32.5 us  [over_axes(): value = jnp.sum(lax.all_gather(value, axis), axis=0)]
    psum x2 -> x0, blocking collectives: 26.1 us -> none  [over_axes(): value = lax.psum(value, axis)]
    all_gather x1, blocking collectives: 19.5 us -> 22.9 us  [body(): modulation = lax.all_gather(summed, 'tp', axis=1, tiled=True)]
  transfers between devices with their start and end apart: 3 -> 3, of which waited for: 2 -> 2; matrix products, arithmetic and copies ran while one was open for 29% -> 28% of each run, Pallas kernels for 0% -> 0%
where the time goes in v1:
time: 299 us; the launch traced here: 298 us
  blocking collectives  110 us (37%)
  waiting for transfers between devices  73 us (24%)
  matrix products  57.2 us (19%)
  other arithmetic  23 us (8%)
  local copies, waits for them, and re-layouts  20.4 us (7%)
  between operations  13.4 us (4%)
    all_gather x1, waiting for transfers between devices, side_by_side(): filled, at, done = (lax.all_gather(both, axis, axis=dim, tiled=True), 0, [])  46.4 us
    all_gather x1, blocking collectives, side_by_side(): filled, at, done = (lax.all_gather(both, axis, axis=dim, tiled=True), 0, [])  40.5 us
    all_gather x2, blocking collectives, over_axes(): value = jnp.sum(lax.all_gather(value, axis), axis=0)  32.5 us
    all_gather x1, waiting for transfers between devices, body(): piece = lax.all_gather(normalised_rows, 'tp', axis=0, tiled=True)  25.9 us
    all_gather x1, blocking collectives, body(): modulation = lax.all_gather(summed, 'tp', axis=1, tiled=True)  22.9 us
    dot_general x8, matrix products, update(): jnp.einsum('hqk,khd->hqd', weights_now.astype(jnp.bfloat16), value_block,...  22.2 us
    dot_general x8, matrix products, update(): jnp.einsum('hqd,khd->hqk', grouped, key_block, preferred_element_type=jnp...  18.4 us
    all_to_all x1, blocking collectives, body(): lax.all_to_all(attended, 'tp', split_axis=0, concat_axis=1, tiled=True)  14.5 us
  transfers between devices with their start and end apart: 3, of which 2 were waited for; matrix products, arithmetic and copies ran while one was open for 28% of the time, Pallas kernels for 0%

profile of v1, /device:TPU:1, one launch (start us, length us, event | category | flops | bytes accessed | tf_op | source)
XLA Modules:
  0.0 297.8 jit_solution(6302469785545887077)
XLA Ops:
  7.8 23.1 %all-gather.2 = f32[8,2,768]{2,1,0:T(2,128)S(1)} all-gather(f32[1,2,768]{2,1,0:T(2,128)S(1)} %convolution_bitcast_fusion.1), channel_id=2, replica_groups=mesh['sp_0'=8,'sp_1'=4,'tp'=8] {'sp_0'}, dimensions={0}, use_global_device_ids=true | all-gather | bytes 55296 | tf_op jit(solution)/shard_map/all_gather | solution.py:17
  30.9 9.4 %all-gather.3 = f32[4,2,768]{2,1,0:T(2,128)S(1)} all-gather(f32[1,2,768]{2,1,0:T(2,128)S(1)} %bitcast.130), channel_id=3, replica_groups=mesh['sp_0'=8,'sp_1'=4,'tp'=8] {'sp_1'}, dimensions={0}, use_global_device_ids=true | all-gather | bytes 30720 | tf_op jit(solution)/shard_map/all_gather | solution.py:17
  40.4 22.9 %all_gather.31 = f32[2,6144]{1,0:T(2,128)S(1)} all-gather(f32[2,768]{1,0:T(2,128)S(1)} %reduce_sum.95), channel_id=1, replica_groups=mesh['sp_0'=8,'sp_1'=4,'tp'=8] {'tp'}, dimensions={1}, use_global_device_ids=true | all-gather | bytes 55296 | tf_op jit(solution)/shard_map/all_gather | solution.py:88
  64.5 1.8 fusion.31
  66.4 25.9 %all-gather.8.cloned.1.call-done = bf16[512,2048]{1,0:T(8,128)(2,1)} async-done(((bf16[64,2048]{1,0:T(8,128)(2,1)}), bf16[512,2048]{1,0:T(8,128)(2,1)}) %all-gather.8.cloned.1.call-update) | async-done | bytes 2097168 | tf_op jit(solution)/shard_map/all_gather | solution.py:94
  92.3 2.5 multiply_reduce_fusion.3
  95.5 2.5 fusion.22
  99.5 3.0 multiply_cosine_fusion.1
  105.4 40.5 %all_gather.33 = bf16[512,2,128]{2,0,1:T(8,128)(2,1)} all-gather(bf16[16,2,128]{2,0,1:T(8,128)(2,1)S(1)} %pad_maximum_fusion.2), channel_id=1, replica_groups=mesh['sp_0'=8,'sp_1'=4,'tp'=8] {'sp_0','sp_1'}, dimensions={0}, use_global_device_ids=true | all-gather | bytes 270336 | tf_op jit(solution)/shard_map/all_gather | solution.py:23
  152.4 46.4 %all-gather.10.cloned.1.call-done = bf16[16384,2,128]{0,2,1:T(8,128)(2,1)} async-done(((bf16[512,2,128]{0,2,1:T(8,128)(2,1)}), bf16[16384,2,128]{0,2,1:T(8,128)(2,1)}) %all-gather.10.cloned.1.call-update) | async-done | bytes 8388624 | tf_op jit(solution)/shard_map/all_gather | solution.py:23
  198.8 5.8 %fusion.75 = (bf16[16384,1,128]{0,2,1:T(8,128)(2,1)}, bf16[16384,1,128]{0,2,1:T(8,128)(2,1)}) fusion(bf16[16384,2,128]{0,2,1:T(8,128)(2,1)} %all-gather.10.cloned.1.call-done), kind=kLoop, calls=%fused_computation.126 | loop fusion | bytes 16777216 | tf_op jit(solution)/shard_map/slice | solution.py:25
  204.6 6.3 %copy.29 = bf16[16384,1,128]{2,0,1:T(8,128)(2,1)} copy(bf16[16384,1,128]{0,2,1:T(8,128)(2,1)} %get-tuple-element.85) | data formatting | bytes 8388608 | tf_op jit(solution)/shard_map/while | solution.py:172
  211.0 6.5 %copy.30 = bf16[16384,1,128]{2,0,1:T(8,128)(2,1)} copy(bf16[16384,1,128]{0,2,1:T(8,128)(2,1)} %get-tuple-element.84) | data formatting | bytes 8388608 | tf_op jit(solution)/shard_map/while | solution.py:172
  217.4 52.6 %while.14 = (s32[]{:T(128)}, f32[1,1024]{1,0:T(1,128)S(1)}, f32[1,1024]{1,0:T(1,128)S(1)}, f32[1,1024,128]{2,1,0:T(8,128)S(1)}, bf16[8,2048,1,128]{3,1,2,0:T(8,1...) while((s32[]{:T(128)}, f32[1,1024]{1,0:T(1,128)S(1)}, ...), condition=%wide.region_12.13_spmd, body=%wide.region_9.12_spmd.sunk | while | flops 1090783232 | bytes 27590756 | solution.py:172
  217.4 2.3 multiply_reduce_fusion.6
  221.2 2.8 fusion.96
  224.0 2.3 multiply_reduce_fusion.6
  227.8 2.8 fusion.96
  230.6 2.3 multiply_reduce_fusion.6
  234.4 2.8 fusion.96
  237.2 2.3 multiply_reduce_fusion.6
  241.0 2.8 fusion.96
  243.8 2.3 multiply_reduce_fusion.6
  247.5 2.8 fusion.96
  250.3 2.3 multiply_reduce_fusion.6
  254.1 2.8 fusion.96
  256.9 2.3 multiply_reduce_fusion.6
  260.7 2.8 fusion.96
  263.5 2.3 multiply_reduce_fusion.6
  267.2 2.8 fusion.96
  270.7 14.5 %all_to_all.19 = bf16[8,64,256]{2,1,0:T(8,128)(2,1)S(1)} all-to-all(bf16[8,64,256]{2,1,0:T(8,128)(2,1)S(1)} %all_to_all.14), channel_id=1, replica_groups=mesh['sp_0'=8,'sp_1'=4,'tp'=8] {'tp'}, dimensions={0} | all-to-all | bytes 524288 | tf_op jit(solution)/shard_map/all_to_all | solution.py:180
  285.3 5.1 %multiply_reduce_fusion.1 = (f32[64]{0:T(128)S(1)}, f32[64,2048]{1,0:T(8,128)S(1)}) fusion(bf16[64,2048]{1,0:T(8,128)(2,1)S(1)} %bitcast.113, bf16[2048,2048]{1,0:T(8,128)(2,1)} %all-gather.12.cloned.1.call-done), kind=kOutput, calls=%fused_computation.40 | convolution fusion | flops 537132992 | bytes 9175296 | tf_op jit(solution)/shard_map/dot_general | solution.py:181
  (87 shorter events, 27.3 us)
Async XLA Ops:
  6.5 139.3 %copy-start = (bf16[2048,256]{1,0:T(8,128)(2,1)S(1)}, bf16[2048,256]{1,0:T(8,128)(2,1)}, u32[]{:S(2)}) copy-start(bf16[2048,256]{1,0:T(8,128)(2,1)} %param.18) | copy-start | bytes 3145732
  6.5 88.3 %copy-start.5 = (f32[128]{0:T(128)S(1)}, f32[128]{0:T(128)}, u32[]{:S(2)}) copy-start(f32[128]{0:T(128)} %param.23) | copy-start | bytes 1540
  6.5 85.7 %all-gather.8.cloned.1.call-start = ((), (), s32[]{:S(2)}) async-start(), calls=%async_computation.1 | async-start | bytes 2359296 | tf_op jit(solution)/shard_map/all_gather | solution.py:94
  66.3 132.5 %all-gather.10.cloned.1.call-start = ((), (), s32[]{:S(2)}) async-start(), calls=%async_computation.2 | async-start | bytes 8650752 | tf_op jit(solution)/shard_map/all_gather | solution.py:23
  66.4 36.1 %copy-start.4 = (bf16[16,2048]{1,0:T(8,128)(2,1)S(1)}, bf16[16,2048]{1,0:T(8,128)(2,1)}, u32[]{:S(2)}) copy-start(bf16[16,2048]{1,0:T(8,128)(2,1)} %param.14) | copy-start | bytes 196612
  94.8 51.1 %copy-start.1 = (bf16[512,2048]{1,0:T(8,128)(2,1)S(1)}, bf16[512,2048]{1,0:T(8,128)(2,1)}, u32[]{:S(2)}) copy-start(bf16[512,2048]{1,0:T(8,128)(2,1)} %all-gather.8.cloned.1.call-done) | copy-start | bytes 6291460
  98.8 50.0 %copy-start.6 = (f32[128]{0:T(128)S(1)}, f32[128]{0:T(128)}, u32[]{:S(2)}) copy-start(f32[128]{0:T(128)} %param.22) | copy-start | bytes 1540
  98.8 186.5 %all-gather.12.cloned.1.call-start = ((), (), s32[]{:S(2)}) async-start(), calls=%async_computation.3 | async-start | bytes 9437184 | tf_op jit(solution)/shard_map/all_gather | solution.py:183
  147.4 3.5 %copy-start.3 = (bf16[512,2,128]{2,0,1:T(8,128)(2,1)S(1)}, bf16[512,2,128]{2,0,1:T(8,128)(2,1)}, u32[]{:S(2)}) copy-start(bf16[512,2,128]{2,0,1:T(8,128)(2,1)} %all_gather.33) | copy-start | bytes 786436
  285.2 5.1 %copy-start.2 = (bf16[64,2048]{1,0:T(8,128)(2,1)S(1)}, bf16[64,2048]{1,0:T(8,128)(2,1)}, u32[]{:S(2)}) copy-start(bf16[64,2048]{1,0:T(8,128)(2,1)} %param.13) | copy-start | bytes 786436
Sparse Core Ops, SparseCore 0:
  66.4 25.8 all-gather.7
  98.9 99.8 all-gather.9
  200.7 54.6 all-gather.11
